TPU v7x, 32 devices: a whole 2x2x4 slice. The times are simulated.
32 devices in a mesh: ep: 8 (over z, y), tp: 4 (over x, core).
Axes of the slice: x: 2, y: 2, z: 4, core: 2. Of those that a mesh axis runs over, the one named last changes fastest.
Arguments:
- tokens: bfloat16 [64, 2048], P('ep'), may hold values from -4 to 4
- w_query: bfloat16 [2048, 1024], P(None, 'tp'), may hold values from -0.125 to 0.125
- w_key: bfloat16 [2048, 1024], P(None, 'tp'), may hold values from -0.125 to 0.125
- w_value: bfloat16 [2048, 1024], P(None, 'tp'), may hold values from -0.125 to 0.125
- w_outgate: bfloat16 [2048, 1024], P(None, 'tp'), may hold values from -0.125 to 0.125
- w_igate: bfloat16 [2048, 4], P(None, 'tp'), may hold values from -0.125 to 0.125
- w_fgate: bfloat16 [2048, 4], P(None, 'tp'), may hold values from -0.125 to 0.125
- forget_bias: float32 [4], P('tp'), may hold values from -1 to 5
- w_out: bfloat16 [1024, 2048], P('tp'), may hold values from -0.1875 to 0.1875
- gain_mix: float32 [2048], replicated, may hold values from 0.1 to 1.9
- gain_moe: float32 [2048], replicated, may hold values from 0.1 to 1.9
- memory: float32 [64, 4, 256, 256], P('ep', 'tp'), may hold values from -0.4 to 0.4
- normalizer: float32 [64, 4, 256], P('ep', 'tp'), may hold values from -0.8 to 0.8
- stabilizer: float32 [64, 4], P('ep', 'tp'), may hold values from 0 to 2
- expert_gate: bfloat16 [8, 2048, 512], P('ep', None, 'tp'), may hold values from -0.125 to 0.125
- expert_up: bfloat16 [8, 2048, 512], P('ep', None, 'tp'), may hold values from -0.125 to 0.125
- expert_down: bfloat16 [8, 512, 2048], P('ep', 'tp'), may hold values from -1 to 1
- routes: int32 [64, 4], P('ep'), may hold values from 0 to 7, all different within a row; in each aligned block of 8 rows (0 to 7, 8 to 15, ...) at most 8 rows name the same one
- route_weight: float32 [64, 4], P('ep'), may hold values from 0.2 to 1
Outputs:
- output: bfloat16 [64, 2048], P('ep', 'tp')
- memory_next: float32 [64, 4, 256, 256], P('ep', 'tp')
- norm_next: float32 [64, 4, 256], P('ep', 'tp')
- stabilizer_next: float32 [64, 4], P('ep', 'tp')
Inputs may be any that keep to these rules, and one draw needn't show every extreme that they name: `routes`: each row names 4 different experts. Among the 8 rows of one device (aligned blocks), no expert is named more than 8 times, a bound that some block reaches.
All inputs are finite; a program needn't handle non-finite values.
Results may differ from a plain program's by a relative error of at most 0.029.
Values may be sent and summed in bfloat16 or wider, within the bound.
No kernel may reach another device: no remote copies, remote signals or barrier semaphores. Data moves between devices by JAX's collectives and lax.ppermute only.
A program may use at most 64 MiB of HBM per device.

v0:
```python
import math
import jax
import jax.numpy as jnp
from jax import lax
from jax.sharding import PartitionSpec as P


def layer_norm(row_data, gain_vec):
    values = row_data.astype(jnp.float32)
    row_mean = jnp.mean(values, -1, keepdims=True)
    centered = values - row_mean
    variance = jnp.mean(centered * centered, -1, keepdims=True)
    return centered * lax.rsqrt(variance + 1e-05) * gain_vec


def slot_targets(routes, experts, capacity):
    flat_routes = routes.reshape(-1)
    onehot = (flat_routes[:, None] == jnp.arange(experts, dtype=jnp.int32)[None, :]).astype(
        jnp.int32
    )
    before = jnp.cumsum(onehot, axis=0) - onehot
    slot_index = jnp.sum(before * onehot, axis=1)
    return flat_routes * capacity + slot_index


def shards(
    tokens,
    w_query,
    w_key,
    w_value,
    w_outgate,
    w_igate,
    w_fgate,
    forget_bias,
    w_out,
    gain_mix,
    gain_moe,
    memory,
    normalizer,
    stabilizer,
    expert_gate,
    expert_up,
    expert_down,
    routes,
    route_weight,
):
    seq_rows = tokens.shape[0]
    model_width = tokens.shape[1]
    head_count = memory.shape[1]
    head_size = memory.shape[2]
    head_cols = head_count * head_size
    normed = layer_norm(tokens, gain_mix).astype(jnp.bfloat16)
    gate_in = jnp.dot(normed, w_igate, preferred_element_type=jnp.float32)
    gate_forget = jnp.dot(normed, w_fgate, preferred_element_type=jnp.float32)
    weights = (w_query, w_key, w_value, w_outgate)
    projected = jnp.concatenate(
        [jnp.dot(normed, weight, preferred_element_type=jnp.float32) for weight in weights], axis=1
    )
    rounded = projected.astype(jnp.bfloat16).reshape(seq_rows, 4, head_count, head_size)
    queries = rounded[:, 0].astype(jnp.float32)
    keys_scaled = rounded[:, 1].astype(jnp.float32) / math.sqrt(head_size)
    values_rows = rounded[:, 2].astype(jnp.float32)
    out_gate = rounded[:, 3].astype(jnp.float32)
    log_forget = jax.nn.log_sigmoid(gate_forget + forget_bias)
    stabilizer_next = jnp.maximum(log_forget + stabilizer, gate_in)
    keep_rate = jnp.exp(log_forget + stabilizer - stabilizer_next)
    admit_rate = jnp.exp(gate_in - stabilizer_next)
    memory_next = (
        keep_rate[:, :, None, None] * memory
        + admit_rate[:, :, None, None] * keys_scaled[:, :, :, None] * values_rows[:, :, None, :]
    )
    norm_next = keep_rate[:, :, None] * normalizer + admit_rate[:, :, None] * keys_scaled
    numerator = jnp.einsum("shk,shkv->shv", queries, memory_next, precision=lax.Precision.HIGHEST)
    denominator = jnp.sum(queries * norm_next, axis=-1)
    readout = numerator / jnp.maximum(jnp.abs(denominator), jnp.exp(-stabilizer_next))[:, :, None]
    mixed = (jax.nn.sigmoid(out_gate) * readout).astype(jnp.bfloat16).reshape(seq_rows, head_cols)
    head_part = jnp.dot(mixed, w_out, preferred_element_type=jnp.float32).astype(jnp.bfloat16)
    summed = lax.psum(head_part, "tp").astype(jnp.float32)
    residual = tokens.astype(jnp.float32) + summed
    expert_in = layer_norm(residual, gain_moe).astype(jnp.bfloat16)
    top_count = routes.shape[1]
    local_experts = expert_gate.shape[0]
    expert_count = local_experts * lax.axis_size("ep")
    capacity = max(2, 2 * seq_rows * top_count // expert_count)
    target = slot_targets(routes, expert_count, capacity)
    outbound = (
        jnp.zeros((expert_count * capacity, model_width), jnp.bfloat16)
        .at[target]
        .set(jnp.repeat(expert_in, top_count, axis=0))
    )
    outbound = outbound.reshape(expert_count, capacity, model_width)
    quarter = model_width // lax.axis_size("tp")
    arrived = lax.all_to_all(outbound, "ep", split_axis=0, concat_axis=0, tiled=True)
    slot_count = arrived.shape[1]
    grouped = arrived.reshape(-1, local_experts, slot_count, model_width)
    gate_part = jnp.einsum(
        "aecd,edf->aecf", grouped, expert_gate, preferred_element_type=jnp.float32
    )
    up_part = jnp.einsum("aecd,edf->aecf", grouped, expert_up, preferred_element_type=jnp.float32)
    hidden = (jax.nn.silu(gate_part) * up_part).astype(jnp.bfloat16)
    partial_value, slot_count = (
        jnp.einsum("aecf,efd->aecd", hidden, expert_down, preferred_element_type=jnp.float32),
        slot_count,
    )
    reduced = lax.psum_scatter(partial_value, "tp", scatter_dimension=3, tiled=True).astype(
        jnp.bfloat16
    )
    reduced = reduced.reshape(-1, slot_count, reduced.shape[3])
    returned = lax.all_to_all(reduced, "ep", split_axis=0, concat_axis=0, tiled=True)
    picked = jnp.take(returned.reshape(expert_count * capacity, quarter), target, axis=0).reshape(
        seq_rows, top_count, quarter
    )
    combined = jnp.sum(route_weight[:, :, None] * picked.astype(jnp.float32), axis=1)
    own_cols = lax.dynamic_slice_in_dim(residual, lax.axis_index("tp") * quarter, quarter, 1)
    output = (own_cols + combined).astype(jnp.bfloat16)
    return (output, memory_next, norm_next, stabilizer_next)


def solution(mesh):
    return jax.shard_map(
        shards,
        mesh=mesh,
        in_specs=(
            P("ep", None),
            P(None, "tp"),
            P(None, "tp"),
            P(None, "tp"),
            P(None, "tp"),
            P(None, "tp"),
            P(None, "tp"),
            P("tp"),
            P("tp", None),
            P(),
            P(),
            P("ep", "tp", None, None),
            P("ep", "tp", None),
            P("ep", "tp"),
            P("ep", None, "tp"),
            P("ep", None, "tp"),
            P("ep", "tp", None),
            P("ep", None),
            P("ep", None),
        ),
        out_specs=(P("ep", "tp"), P("ep", "tp", None, None), P("ep", "tp", None), P("ep", "tp")),
        check_vma=False,
    )
```

profile of v0, /device:TPU:0, one launch (start us, length us, event | category | flops | bytes accessed | tf_op | source)
XLA Modules:
  0.0 94.1 jit_solution(10027938302184542748)
XLA Ops:
  7.2 0.9 copy.30
  8.1 0.1 reshape.339
  8.2 1.0 %convert_reduce_fusion = f32[8]{0:T(128)S(1)} fusion(bf16[8,2048]{1,0:T(8,128)(2,1)} %param.19), kind=kLoop, calls=%fused_computation.36 | loop fusion | flops 32760 | bytes 32800 | tf_op jit(solution)/shard_map/reduce_sum | solution.py:10
  9.3 1.0 %fusion.24 = f32[8]{0:T(128)S(1)} fusion(bf16[8,2048]{1,0:T(8,128)(2,1)} %param.19, f32[8]{0:T(128)S(1)} %broadcast_multiply_fusion.3), kind=kLoop, calls=%fused_computation.39 | loop fusion | flops 65528 | bytes 32832 | tf_op jit(solution)/shard_map/reduce_sum | solution.py:12
  10.9 0.8 fusion.26
  11.7 0.8 convolution_bitcast_fusion.3
  12.6 0.8 exponential_bitcast_fusion
  13.4 1.5 %fusion.5 = f32[8,256]{1,0:T(8,128)S(1)} fusion(bf16[8,2048]{1,0:T(8,128)(2,1)S(1)} %fusion.26, bf16[2048,256]{1,0:T(8,128)(2,1)} %param.22), kind=kOutput, calls=%fused_computation.13 | convolution fusion | flops 8392704 | bytes 1089536 | tf_op jit(solution)/shard_map/dot_general | solution.py:57
  14.9 1.4 %broadcast_multiply_fusion = (f32[8,256]{1,0:T(8,128)S(1)}, f32[8,256]{1,0:T(8,128)S(1)}) fusion(f32[8]{0:T(128)S(1)} %multiply_bitcast_fusion, bf16[8,2048]{1,0:T(8,128)(2,1)S(1)} %fusion.26, bf16[2048,256]{1,0:T(8,128)(2,1)} %param.21), kind=kOutput, calls=%fused_computation.68 | convolution fusion | flops 8394752 | bytes 1097760 | tf_op jit(solution)/shard_map/dot_general | solution.py:57
  16.4 0.4 fusion.34
  16.8 0.5 multiply_add_fusion
  17.3 0.8 fusion
  18.1 2.0 %convolution_convert_fusion = bf16[8,2048]{1,0:T(8,128)(2,1)S(1)} fusion(bf16[256,2048]{1,0:T(8,128)(2,1)S(1)} %copy-done, bf16[8,2048]{1,0:T(8,128)(2,1)S(1)} %fusion.26, bf16[2048,256]{1,0:T(8,128)(2,1)} %param.23, f32[8,1,256]{2,1,0:T(1,128)S(1)} %fusion, f32[8]{0:T(128)S(1)} %fusion.42), kind=kOutput, calls=%fused_computation.3 | convolution fusion | flops 16809984 | bytes 2170912 | tf_op jit(solution)/shard_map/dot_general | solution.py:77
  20.1 12.9 %psum.7 = bf16[8,2048]{1,0:T(8,128)(2,1)S(1)} all-reduce(bf16[8,2048]{1,0:T(8,128)(2,1)S(1)} %convolution_convert_fusion), channel_id=1, replica_groups=mesh['ep'=8,'tp'=4] {'tp'}, use_global_device_ids=true, to_apply=%region_3.4 | all-reduce | flops 16384 | bytes 65536 | tf_op jit(solution)/shard_map/psum | solution.py:78
  33.0 0.1 convert_add_fusion
  33.2 0.2 multiply_reduce_fusion.1
  33.4 0.1 multiply_convert_fusion
  33.7 0.2 select_reduce_fusion
  33.9 0.1 mul.192
  34.0 0.9 scatter_custom_fusion
  34.9 13.9 %all_to_all.10 = bf16[8,8,2048]{2,1,0:T(8,128)(2,1)S(1)} all-to-all(bf16[8,8,2048]{2,1,0:T(8,128)(2,1)S(1)} %bitcast.115), channel_id=1, replica_groups=mesh['ep'=8,'tp'=4] {'ep'}, dimensions={0} | all-to-all | bytes 524288 | tf_op jit(solution)/shard_map/all_to_all | solution.py:93
  48.7 1.3 %convolution_bitcast_fusion.2 = f32[8,1,8,128]{3,2,0,1:T(8,128)S(1)} fusion(bf16[8,8,2048]{2,1,0:T(8,128)(2,1)S(1)} %all_to_all.10, bf16[1,2048,128]{2,1,0:T(8,128)(2,1)} %param.33), kind=kOutput, calls=%fused_computation.9 | convolution fusion | flops 33554432 | bytes 819200 | tf_op jit(solution)/shard_map/aecd,edf->aecf/dot_general | solution.py:96
  50.0 1.2 %convolution_bitcast_fusion = f32[8,1,8,2048]{3,2,0,1:T(8,128)} fusion(bf16[8,8,2048]{2,1,0:T(8,128)(2,1)S(1)} %all_to_all.10, bf16[1,128,2048]{2,1,0:T(8,128)(2,1)S(1)} %copy-done.5, bf16[1,2048,128]{2,1,0:T(8,128)(2,1)S(1)} %copy-done.6, f32[8,1,8,128]{3,2,0,1:T(8,128)S(1)} %convolution_bitcast_fusion.2), kind=kOutput, calls=%fused_computation.2 | convolution fusion | flops 67158016 | bytes 1867776 | tf_op jit(solution)/shard_map/aecf,efd->aecd/dot_general | solution.py:102
  51.3 20.7 %reduce-scatter.2.cloned.1.call-done = f32[8,1,8,512]{3,2,0,1:T(8,128)} async-done(((f32[8,1,8,2048]{3,2,0,1:T(8,128)}), f32[8,1,8,512]{3,2,0,1:T(8,128)}) %reduce-scatter.2.cloned.1.call-update) | async-done | bytes 131088 | tf_op jit(solution)/shard_map/reduce_scatter | solution.py:105
  72.0 1.5 %convert_bitcast_fusion = bf16[8,8,512]{2,1,0:T(8,128)(2,1)} fusion(f32[8,1,8,512]{3,2,0,1:T(8,128)} %reduce-scatter.2.cloned.1.call-done), kind=kLoop, calls=%fused_computation.43 | loop fusion | flops 32768 | bytes 196608 | tf_op jit(solution)/shard_map/reshape | solution.py:108
  73.5 5.5 %all-to-all-start.1 = ((bf16[8,8,512]{2,1,0:T(8,128)(2,1)}), bf16[8,8,512]{2,1,0:T(8,128)(2,1)S(1)}, u32[]{:S(2)}, u32[]{:S(2)}) async-start(bf16[8,8,512]{2,1,0:T(8,128)(2,1)} %convert_bitcast_fusion), calls=%async_computation.2 | async-start | bytes 131072 | tf_op jit(solution)/shard_map/all_to_all | solution.py:109
  79.0 0.1 copy.29
  79.1 0.6 copy.32
  79.7 6.2 %all-to-all-done.1 = bf16[8,8,512]{2,1,0:T(8,128)(2,1)S(1)} async-done(((bf16[8,8,512]{2,1,0:T(8,128)(2,1)}), bf16[8,8,512]{2,1,0:T(8,128)(2,1)S(1)}, u32[]{:S(2)}, u32[]{:S(2)}) %all-to-all-start.1) | async-done | bytes 65568 | tf_op jit(solution)/shard_map/all_to_all | solution.py:109
  85.9 0.6 gather_fusion
  86.6 0.1 multiply_reduce_fusion
  86.7 0.6 add_convert_fusion
  (40 shorter events, 0.5 us)
Async XLA Ops:
  7.2 11.0 %copy-start = (bf16[256,2048]{1,0:T(8,128)(2,1)S(1)}, bf16[256,2048]{1,0:T(8,128)(2,1)}, u32[]{:S(2)}) copy-start(bf16[256,2048]{1,0:T(8,128)(2,1)} %param.27) | copy-start | bytes 3145732
  7.2 9.2 %copy-start.4 = (bf16[2048,256]{1,0:T(8,128)(2,1)S(1)}, bf16[2048,256]{1,0:T(8,128)(2,1)}, u32[]{:S(2)}) copy-start(bf16[2048,256]{1,0:T(8,128)(2,1)} %param.20) | copy-start | bytes 3145732
  7.2 9.2 %copy-start.7 = (f32[8,1,256]{2,1,0:T(1,128)S(1)}, f32[8,1,256]{2,1,0:T(1,128)}, u32[]{:S(2)}) copy-start(f32[8,1,256]{2,1,0:T(1,128)} %param.31) | copy-start | bytes 24580
  7.2 64.8 %reduce-scatter.2.cloned.1.call-start = ((), (), s32[]{:S(2)}) async-start(), calls=%async_computation.3 | async-start | bytes 655360 | tf_op jit(solution)/shard_map/reduce_scatter | solution.py:105
  8.2 8.6 %copy-start.2 = (f32[8,1,256,256]{3,2,1,0:T(8,128)S(1)}, f32[8,1,256,256]{3,2,1,0:T(8,128)}, u32[]{:S(2)}) copy-start(f32[8,1,256,256]{3,2,1,0:T(8,128)} %param.30) | copy-start | bytes 6291460
  13.4 3.8 %copy-start.10 = (f32[8,1]{0,1:T(1,128)}, f32[8,1]{0,1:T(1,128)S(1)}, u32[]{:S(2)}) copy-start(f32[8,1]{0,1:T(1,128)S(1)} %get-tuple-element.15) | copy-start | bytes 100
  17.3 2.8 %copy-start.1 = (f32[8,1,256,256]{3,2,1,0:T(8,128)}, f32[8,1,256,256]{3,2,1,0:T(8,128)S(1)}, u32[]{:S(2)}) copy-start(f32[8,1,256,256]{3,2,1,0:T(8,128)S(1)} %multiply_add_fusion) | copy-start | bytes 6291460
  17.3 15.7 %copy-start.3 = (bf16[8,2048]{1,0:T(8,128)(2,1)S(1)}, bf16[8,2048]{1,0:T(8,128)(2,1)}, u32[]{:S(2)}) copy-start(bf16[8,2048]{1,0:T(8,128)(2,1)} %param.19) | copy-start | bytes 98308
  17.3 16.1 %copy-start.8 = (f32[2048]{0:T(1024)S(1)}, f32[2048]{0:T(1024)}, u32[]{:S(2)}) copy-start(f32[2048]{0:T(1024)} %param.29) | copy-start | bytes 24580
  33.0 17.0 %copy-start.5 = (bf16[1,128,2048]{2,1,0:T(8,128)(2,1)S(1)}, bf16[1,128,2048]{2,1,0:T(8,128)(2,1)}, u32[]{:S(2)}) copy-start(bf16[1,128,2048]{2,1,0:T(8,128)(2,1)} %param.35) | copy-start | bytes 1572868
  33.0 17.0 %copy-start.6 = (bf16[1,2048,128]{2,1,0:T(8,128)(2,1)S(1)}, bf16[1,2048,128]{2,1,0:T(8,128)(2,1)}, u32[]{:S(2)}) copy-start(bf16[1,2048,128]{2,1,0:T(8,128)(2,1)} %param.34) | copy-start | bytes 1572868
  34.9 44.2 %copy-start.9 = (f32[8,4]{0,1:T(4,128)S(1)}, f32[8,4]{0,1:T(4,128)}, u32[]{:S(2)}) copy-start(f32[8,4]{0,1:T(4,128)} %param.37) | copy-start | bytes 388
  73.5 12.4 %all-to-all-start.1 = ((bf16[8,8,512]{2,1,0:T(8,128)(2,1)}), bf16[8,8,512]{2,1,0:T(8,128)(2,1)S(1)}, u32[]{:S(2)}, u32[]{:S(2)}) async-start(bf16[8,8,512]{2,1,0:T(8,128)(2,1)} %convert_bitcast_fusion), calls=%async_computation.2 | async-start | bytes 131072 | tf_op jit(solution)/shard_map/all_to_all | solution.py:109
Sparse Core Ops, SparseCore 0:
  51.3 20.5 reduce-scatter.1
where the time goes:
time: 94.8 us; the launch traced here: 94.1 us
  waiting for transfers between devices  26.9 us (28%)
  blocking collectives  26.8 us (28%)
  between operations  14.9 us (16%)
  matrix products  10.2 us (11%)
  other arithmetic  6.35 us (7%)
  starting transfers between devices  5.55 us (6%)
  local copies, waits for them, and re-layouts  3.52 us (4%)
    reduce_scatter x1, waiting for transfers between devices, shards(): lax.psum_scatter(partial_value, 'tp', scatter_dimension=3, tiled=True)  20.7 us
    all_to_all x1, blocking collectives, shards(): lax.all_to_all(outbound, 'ep', split_axis=0, concat_axis=0, tiled=True)  13.9 us
    psum x1, blocking collectives, shards(): summed = lax.psum(head_part, 'tp').astype(jnp.float32)  12.9 us
    all_to_all x1, waiting for transfers between devices, shards(): lax.all_to_all(reduced, 'ep', split_axis=0, concat_axis=0, tiled=True)  6.19 us
    all_to_all x1, starting transfers between devices, shards(): lax.all_to_all(reduced, 'ep', split_axis=0, concat_axis=0, tiled=True)  5.52 us
    dot_general x3, matrix products, shards(): jnp.dot(normed, weight, preferred_element_type=jnp.float32)  3.27 us
    dot_general x1, matrix products, shards(): jnp.dot(mixed, w_out, preferred_element_type=jnp.float32)  1.96 us
  transfers between devices with their start and end apart: 2, of which 2 were waited for; matrix products, arithmetic and copies ran while one was open for 1% of the time, Pallas kernels for 0%

commit v1 on v0

--- a/solution.py
+++ b/solution.py
@@ -75,7 +75,7 @@
     readout = numerator / jnp.maximum(jnp.abs(denominator), jnp.exp(-stabilizer_next))[:, :, None]
     mixed = (jax.nn.sigmoid(out_gate) * readout).astype(jnp.bfloat16).reshape(seq_rows, head_cols)
     head_part = jnp.dot(mixed, w_out, preferred_element_type=jnp.float32).astype(jnp.bfloat16)
-    summed = lax.psum(head_part, "tp").astype(jnp.float32)
+    summed = jnp.sum(lax.all_gather(head_part, "tp"), axis=0).astype(jnp.float32)
     residual = tokens.astype(jnp.float32) + summed
     expert_in = layer_norm(residual, gain_moe).astype(jnp.bfloat16)
     top_count = routes.shape[1]

time: 94.8 us -> 90 us (0.949)
  blocking collectives: 26.8 us -> 22 us
    psum x1 -> x0, blocking collectives: 12.9 us -> none  [shards(): summed = lax.psum(head_part, 'tp').astype(jnp.float32)]
    all_gather x0 -> x1, blocking collectives: none -> 6.51 us  [shards(): lax.all_gather(head_part, 'tp')]
    all_to_all x1, blocking collectives: 13.9 us -> 15.4 us  [shards(): lax.all_to_all(outbound, 'ep', split_axis=0, concat_axis=0, tiled=True)]
where the time goes in v1:
time: 90 us; the launch traced here: 89.4 us
  waiting for transfers between devices  26.9 us (30%)
  blocking collectives  22 us (24%)
  between operations  14.9 us (17%)
  matrix products  10.2 us (11%)
  other arithmetic  6.37 us (7%)
  starting transfers between devices  5.56 us (6%)
  local copies, waits for them, and re-layouts  3.51 us (4%)
    reduce_scatter x1, waiting for transfers between devices, shards(): lax.psum_scatter(partial_value, 'tp', scatter_dimension=3, tiled=True)  20.7 us
    all_to_all x1, blocking collectives, shards(): lax.all_to_all(outbound, 'ep', split_axis=0, concat_axis=0, tiled=True)  15.4 us
    all_gather x1, blocking collectives, shards(): lax.all_gather(head_part, 'tp')  6.51 us
    all_to_all x1, waiting for transfers between devices, shards(): lax.all_to_all(reduced, 'ep', split_axis=0, concat_axis=0, tiled=True)  6.19 us
    all_to_all x1, starting transfers between devices, shards(): lax.all_to_all(reduced, 'ep', split_axis=0, concat_axis=0, tiled=True)  5.52 us
    dot_general x3, matrix products, shards(): jnp.dot(normed, weight, preferred_element_type=jnp.float32)  3.27 us
    dot_general x1, matrix products, shards(): jnp.dot(mixed, w_out, preferred_element_type=jnp.float32)  1.96 us
  transfers between devices with their start and end apart: 2, of which 2 were waited for; matrix products, arithmetic and copies ran while one was open for 1% of the time, Pallas kernels for 0%

profile of v1, /device:TPU:0, one launch (start us, length us, event | category | flops | bytes accessed | tf_op | source)
XLA Modules:
  0.0 89.4 jit_solution(1957538643711558572)
XLA Ops:
  7.2 0.9 copy.30
  8.1 0.1 reshape.339
  8.2 1.0 %convert_reduce_fusion = f32[8]{0:T(128)S(1)} fusion(bf16[8,2048]{1,0:T(8,128)(2,1)} %param.19), kind=kLoop, calls=%fused_computation.37 | loop fusion | flops 32760 | bytes 32800 | tf_op jit(solution)/shard_map/reduce_sum | solution.py:10
  9.3 1.0 %fusion.24 = f32[8]{0:T(128)S(1)} fusion(bf16[8,2048]{1,0:T(8,128)(2,1)} %param.19, f32[8]{0:T(128)S(1)} %broadcast_multiply_fusion.3), kind=kLoop, calls=%fused_computation.40 | loop fusion | flops 65528 | bytes 32832 | tf_op jit(solution)/shard_map/reduce_sum | solution.py:12
  10.9 0.8 fusion.26
  11.7 0.8 convolution_bitcast_fusion.3
  12.6 0.8 exponential_bitcast_fusion
  13.4 1.5 %fusion.5 = f32[8,256]{1,0:T(8,128)S(1)} fusion(bf16[8,2048]{1,0:T(8,128)(2,1)S(1)} %fusion.26, bf16[2048,256]{1,0:T(8,128)(2,1)} %param.22), kind=kOutput, calls=%fused_computation.13 | convolution fusion | flops 8392704 | bytes 1089536 | tf_op jit(solution)/shard_map/dot_general | solution.py:57
  14.9 1.4 %broadcast_multiply_fusion = (f32[8,256]{1,0:T(8,128)S(1)}, f32[8,256]{1,0:T(8,128)S(1)}) fusion(f32[8]{0:T(128)S(1)} %multiply_bitcast_fusion, bf16[8,2048]{1,0:T(8,128)(2,1)S(1)} %fusion.26, bf16[2048,256]{1,0:T(8,128)(2,1)} %param.21), kind=kOutput, calls=%fused_computation.69 | convolution fusion | flops 8394752 | bytes 1097760 | tf_op jit(solution)/shard_map/dot_general | solution.py:57
  16.4 0.4 fusion.34
  16.8 0.5 multiply_add_fusion
  17.3 0.8 fusion
  18.1 2.0 %convolution_convert_fusion = bf16[8,2048]{1,0:T(8,128)(2,1)S(1)} fusion(bf16[256,2048]{1,0:T(8,128)(2,1)S(1)} %copy-done, bf16[8,2048]{1,0:T(8,128)(2,1)S(1)} %fusion.26, bf16[2048,256]{1,0:T(8,128)(2,1)} %param.23, f32[8,1,256]{2,1,0:T(1,128)S(1)} %fusion, f32[8]{0:T(128)S(1)} %fusion.42), kind=kOutput, calls=%fused_computation.3 | convolution fusion | flops 16809984 | bytes 2170912 | tf_op jit(solution)/shard_map/dot_general | solution.py:77
  20.1 6.5 %all-gather = bf16[32,2048]{1,0:T(8,128)(2,1)S(1)} all-gather(bf16[8,2048]{1,0:T(8,128)(2,1)S(1)} %convolution_convert_fusion), channel_id=2, replica_groups=mesh['ep'=8,'tp'=4] {'tp'}, dimensions={0}, use_global_device_ids=true | all-gather | bytes 163840 | tf_op jit(solution)/shard_map/all_gather | solution.py:78
  26.6 0.1 convert_add_fusion
  26.8 0.2 multiply_reduce_fusion.1
  27.0 0.1 multiply_convert_fusion
  27.3 0.2 select_reduce_fusion
  27.5 0.1 mul.192
  27.6 0.9 scatter_custom_fusion
  28.5 15.4 %all_to_all.10 = bf16[8,8,2048]{2,1,0:T(8,128)(2,1)S(1)} all-to-all(bf16[8,8,2048]{2,1,0:T(8,128)(2,1)S(1)} %bitcast.117), channel_id=1, replica_groups=mesh['ep'=8,'tp'=4] {'ep'}, dimensions={0} | all-to-all | bytes 524288 | tf_op jit(solution)/shard_map/all_to_all | solution.py:93
  43.9 1.3 %convolution_bitcast_fusion.2 = f32[8,1,8,128]{3,2,0,1:T(8,128)S(1)} fusion(bf16[8,8,2048]{2,1,0:T(8,128)(2,1)S(1)} %all_to_all.10, bf16[1,2048,128]{2,1,0:T(8,128)(2,1)} %param.33), kind=kOutput, calls=%fused_computation.9 | convolution fusion | flops 33554432 | bytes 819200 | tf_op jit(solution)/shard_map/aecd,edf->aecf/dot_general | solution.py:96
  45.2 1.2 %convolution_bitcast_fusion = f32[8,1,8,2048]{3,2,0,1:T(8,128)} fusion(bf16[8,8,2048]{2,1,0:T(8,128)(2,1)S(1)} %all_to_all.10, bf16[1,128,2048]{2,1,0:T(8,128)(2,1)S(1)} %copy-done.5, bf16[1,2048,128]{2,1,0:T(8,128)(2,1)S(1)} %copy-done.6, f32[8,1,8,128]{3,2,0,1:T(8,128)S(1)} %convolution_bitcast_fusion.2), kind=kOutput, calls=%fused_computation.2 | convolution fusion | flops 67158016 | bytes 1867776 | tf_op jit(solution)/shard_map/aecf,efd->aecd/dot_general | solution.py:102
  46.5 20.7 %reduce-scatter.2.cloned.1.call-done = f32[8,1,8,512]{3,2,0,1:T(8,128)} async-done(((f32[8,1,8,2048]{3,2,0,1:T(8,128)}), f32[8,1,8,512]{3,2,0,1:T(8,128)}) %reduce-scatter.2.cloned.1.call-update) | async-done | bytes 131088 | tf_op jit(solution)/shard_map/reduce_scatter | solution.py:105
  67.2 1.5 %convert_bitcast_fusion = bf16[8,8,512]{2,1,0:T(8,128)(2,1)} fusion(f32[8,1,8,512]{3,2,0,1:T(8,128)} %reduce-scatter.2.cloned.1.call-done), kind=kLoop, calls=%fused_computation.44 | loop fusion | flops 32768 | bytes 196608 | tf_op jit(solution)/shard_map/reshape | solution.py:108
  68.7 5.5 %all-to-all-start.1 = ((bf16[8,8,512]{2,1,0:T(8,128)(2,1)}), bf16[8,8,512]{2,1,0:T(8,128)(2,1)S(1)}, u32[]{:S(2)}, u32[]{:S(2)}) async-start(bf16[8,8,512]{2,1,0:T(8,128)(2,1)} %convert_bitcast_fusion), calls=%async_computation.2 | async-start | bytes 131072 | tf_op jit(solution)/shard_map/all_to_all | solution.py:109
  74.3 0.1 copy.29
  74.4 0.6 copy.32
  75.0 6.2 %all-to-all-done.1 = bf16[8,8,512]{2,1,0:T(8,128)(2,1)S(1)} async-done(((bf16[8,8,512]{2,1,0:T(8,128)(2,1)}), bf16[8,8,512]{2,1,0:T(8,128)(2,1)S(1)}, u32[]{:S(2)}, u32[]{:S(2)}) %all-to-all-start.1) | async-done | bytes 65568 | tf_op jit(solution)/shard_map/all_to_all | solution.py:109
  81.2 0.6 gather_fusion
  81.8 0.1 multiply_reduce_fusion
  81.9 0.6 add_convert_fusion
  (41 shorter events, 0.5 us)
Async XLA Ops:
  7.2 11.0 %copy-start = (bf16[256,2048]{1,0:T(8,128)(2,1)S(1)}, bf16[256,2048]{1,0:T(8,128)(2,1)}, u32[]{:S(2)}) copy-start(bf16[256,2048]{1,0:T(8,128)(2,1)} %param.27) | copy-start | bytes 3145732
  7.2 9.2 %copy-start.4 = (bf16[2048,256]{1,0:T(8,128)(2,1)S(1)}, bf16[2048,256]{1,0:T(8,128)(2,1)}, u32[]{:S(2)}) copy-start(bf16[2048,256]{1,0:T(8,128)(2,1)} %param.20) | copy-start | bytes 3145732
  7.2 9.2 %copy-start.7 = (f32[8,1,256]{2,1,0:T(1,128)S(1)}, f32[8,1,256]{2,1,0:T(1,128)}, u32[]{:S(2)}) copy-start(f32[8,1,256]{2,1,0:T(1,128)} %param.31) | copy-start | bytes 24580
  7.2 60.0 %reduce-scatter.2.cloned.1.call-start = ((), (), s32[]{:S(2)}) async-start(), calls=%async_computation.3 | async-start | bytes 655360 | tf_op jit(solution)/shard_map/reduce_scatter | solution.py:105
  8.2 8.6 %copy-start.2 = (f32[8,1,256,256]{3,2,1,0:T(8,128)S(1)}, f32[8,1,256,256]{3,2,1,0:T(8,128)}, u32[]{:S(2)}) copy-start(f32[8,1,256,256]{3,2,1,0:T(8,128)} %param.30) | copy-start | bytes 6291460
  13.4 3.8 %copy-start.10 = (f32[8,1]{0,1:T(1,128)}, f32[8,1]{0,1:T(1,128)S(1)}, u32[]{:S(2)}) copy-start(f32[8,1]{0,1:T(1,128)S(1)} %get-tuple-element.15) | copy-start | bytes 100
  17.3 2.8 %copy-start.1 = (f32[8,1,256,256]{3,2,1,0:T(8,128)}, f32[8,1,256,256]{3,2,1,0:T(8,128)S(1)}, u32[]{:S(2)}) copy-start(f32[8,1,256,256]{3,2,1,0:T(8,128)S(1)} %multiply_add_fusion) | copy-start | bytes 6291460
  17.3 9.3 %copy-start.3 = (bf16[8,2048]{1,0:T(8,128)(2,1)S(1)}, bf16[8,2048]{1,0:T(8,128)(2,1)}, u32[]{:S(2)}) copy-start(bf16[8,2048]{1,0:T(8,128)(2,1)} %param.19) | copy-start | bytes 98308
  17.3 9.7 %copy-start.8 = (f32[2048]{0:T(1024)S(1)}, f32[2048]{0:T(1024)}, u32[]{:S(2)}) copy-start(f32[2048]{0:T(1024)} %param.29) | copy-start | bytes 24580
  26.6 18.6 %copy-start.5 = (bf16[1,128,2048]{2,1,0:T(8,128)(2,1)S(1)}, bf16[1,128,2048]{2,1,0:T(8,128)(2,1)}, u32[]{:S(2)}) copy-start(bf16[1,128,2048]{2,1,0:T(8,128)(2,1)} %param.35) | copy-start | bytes 1572868
  26.6 18.6 %copy-start.6 = (bf16[1,2048,128]{2,1,0:T(8,128)(2,1)S(1)}, bf16[1,2048,128]{2,1,0:T(8,128)(2,1)}, u32[]{:S(2)}) copy-start(bf16[1,2048,128]{2,1,0:T(8,128)(2,1)} %param.34) | copy-start | bytes 1572868
  28.5 45.8 %copy-start.9 = (f32[8,4]{0,1:T(4,128)S(1)}, f32[8,4]{0,1:T(4,128)}, u32[]{:S(2)}) copy-start(f32[8,4]{0,1:T(4,128)} %param.37) | copy-start | bytes 388
  68.7 12.4 %all-to-all-start.1 = ((bf16[8,8,512]{2,1,0:T(8,128)(2,1)}), bf16[8,8,512]{2,1,0:T(8,128)(2,1)S(1)}, u32[]{:S(2)}, u32[]{:S(2)}) async-start(bf16[8,8,512]{2,1,0:T(8,128)(2,1)} %convert_bitcast_fusion), calls=%async_computation.2 | async-start | bytes 131072 | tf_op jit(solution)/shard_map/all_to_all | solution.py:109
Sparse Core Ops, SparseCore 0:
  46.5 20.6 reduce-scatter.1
